TPU v7x, 512 devices: a whole 4x4x16 slice. The times are simulated.
512 devices in a mesh: ep: 128 (over z, x, core), tp: 4 (over y).
Axes of the slice: x: 4, y: 4, z: 16, core: 2. Of those that a mesh axis runs over, the one named last changes fastest.
Arguments:
- tokens: bfloat16 [16384, 2048], P('ep'), may hold values from -6 to 6
- norm_gain: float32 [2048], replicated, may hold values from 0.1 to 1.9
- expert_ids: int32 [16384, 2], P('ep'), may hold values from 0 to 31, all different within a row; in each aligned block of 128 rows (0 to 127, 128 to 255, ...) at most 12 rows name the same one
- gate_weights: float32 [16384, 2], P('ep'), may hold values from 0.2 to 1
- w_gate: bfloat16 [2048, 131072], P(None, ('ep', 'tp')), may hold values from -0.125 to 0.125
- w_up: bfloat16 [2048, 131072], P(None, ('ep', 'tp')), may hold values from -0.125 to 0.125
- w_down: bfloat16 [131072, 2048], P('ep', 'tp'), may hold values from -0.09375 to 0.09375
Outputs:
- moe_out: bfloat16 [16384, 2048], P('ep', 'tp')
Inputs may be any that keep to these rules, and one draw needn't show every extreme that they name: `expert_ids`: each token names 2 different experts; in each aligned block of 128 rows no expert is named by more than 12 rows, a bound that some block reaches.
All inputs are finite; a program needn't handle non-finite values.
Results may differ from a plain program's by a relative error of at most 0.0071.
Values may be sent and summed in bfloat16 or wider, within the bound.
No kernel may reach another device: no remote copies, remote signals or barrier semaphores. Data moves between devices by JAX's collectives and lax.ppermute only.
A program may use at most 64 MiB of HBM per device.

v0:
```python
import jax
import jax.numpy as jnp
from jax import lax
from jax.sharding import Mesh
from jax.sharding import PartitionSpec as P

TOP = 2
EP = ("ep_0", "ep_1", "ep_2")
EP_TP = ("ep_0", "ep_1", "ep_2", "tp")
EPS = 1e-06


def split_up(array, dim, length):
    lengths = array.shape
    parts = array.reshape(*lengths[:dim], length, lengths[dim] // length, *lengths[dim + 1 :])
    return jnp.moveaxis(parts, dim, 0)


def laid_out(parts, dim):
    parts = jnp.moveaxis(parts, 0, dim)
    lengths = parts.shape
    return parts.reshape(*lengths[:dim], lengths[dim] * lengths[dim + 1], *lengths[dim + 2 :])


def turned_blocks(parts, axes, sequence):
    inside = parts.shape[1:]
    out = parts.reshape(*(lax.axis_size(a) for a in axes), *inside)
    for k in sequence:
        out = lax.all_to_all(out, axes[k], k, k, tiled=True)
    return out.reshape(-1, *inside)


def exchange_by_chip(array, groups, sequence, split_dim, concat_dim):
    length = lax.axis_size(groups[0]) * lax.axis_size(groups[1])
    parts = split_up(array, split_dim, length)
    return laid_out(turned_blocks(parts, groups, sequence), concat_dim)


def rms_rows(values, gain):
    widened = values.astype(jnp.float32)
    scale = lax.rsqrt(jnp.mean(widened * widened, axis=-1, keepdims=True) + EPS)
    return (widened * scale * gain).astype(jnp.bfloat16)


def on_device(tokens, norm_gain, expert_ids, gate_weights, w_gate, w_up, w_down):
    ep_count = lax.axis_size(EP)
    tp_count = lax.axis_size("tp")
    row_count = tokens.shape[0]
    group_size = max(1, ep_count // 32)
    expert_count = ep_count // group_size
    share = (row_count * TOP * 5 + 4 * expert_count * tp_count - 1) // (4 * expert_count * tp_count)
    capacity = min(row_count, tp_count * share)
    normed = rms_rows(tokens, norm_gain)
    flat_ids = expert_ids.reshape(-1)
    matches = (flat_ids[:, None] == jnp.arange(expert_count, dtype=jnp.int32)[None, :]).astype(
        jnp.int32
    )
    slot_index = jnp.sum((jnp.cumsum(matches, axis=0) - matches) * matches, axis=1)
    position = flat_ids * capacity + slot_index
    placing = (
        position[:, None] == jnp.arange(expert_count * capacity, dtype=jnp.int32)[None, :]
    ).astype(jnp.float32)
    placing = placing.reshape(row_count, TOP, expert_count * capacity)
    selector = jnp.sum(placing, axis=1).astype(jnp.bfloat16)
    buffers = lax.dot_general(
        selector, normed, (((0,), (0,)), ((), ())), preferred_element_type=jnp.float32
    )
    buffers = buffers.astype(jnp.bfloat16).reshape(expert_count, capacity, -1)
    quarter = capacity // tp_count
    mine = lax.dynamic_slice_in_dim(buffers, lax.axis_index("tp") * quarter, quarter, 1)
    copies = jnp.repeat(mine, group_size, axis=0)
    arrived = exchange_by_chip(copies, (("ep_0", "ep_1"), "ep_2"), (1, 0), 0, 0)
    received = lax.all_gather(arrived, "tp", axis=1, tiled=True)
    sources, slot_count, model_width = received.shape
    flat_rows = received.reshape(sources * slot_count, model_width)
    gate_proj = jnp.dot(flat_rows, w_gate, preferred_element_type=jnp.float32)
    upper = jnp.dot(flat_rows, w_up, preferred_element_type=jnp.float32)
    hidden = (jax.nn.silu(gate_proj) * upper).astype(jnp.bfloat16)
    partial_out = jnp.dot(
        lax.all_gather(hidden, "tp", axis=1, tiled=True), w_down, preferred_element_type=jnp.float32
    ).astype(jnp.bfloat16)
    partial_out = partial_out.reshape(sources, slot_count, w_down.shape[1])
    sources, slot_count, out_width = partial_out.shape
    back = exchange_by_chip(partial_out, (("ep_0", "ep_1"), "ep_2"), (1, 0), 0, 0)
    back = back.reshape(expert_count, group_size, slot_count, out_width).astype(jnp.float32)
    returned = jnp.sum(back, axis=1)
    summed = returned.reshape(expert_count * capacity, -1)
    combine = jnp.sum(placing * gate_weights[:, :, None], axis=1)
    mixed = jnp.dot(
        combine, summed, precision=lax.Precision.HIGHEST, preferred_element_type=jnp.float32
    )
    return mixed.astype(jnp.bfloat16)


def solution(mesh):
    finer = Mesh(mesh.devices.reshape(16, 4, 2, mesh.shape["tp"]), ("ep_0", "ep_1", "ep_2", "tp"))
    placed = (
        P(EP, None),
        P(),
        P(EP, None),
        P(EP, None),
        P(None, EP_TP),
        P(None, EP_TP),
        P(EP, "tp"),
    )
    return jax.shard_map(
        on_device, mesh=finer, in_specs=placed, out_specs=P(EP, "tp"), check_vma=False
    )
```

profile of v0, /device:TPU:2, one launch (start us, length us, event | category | flops | bytes accessed | tf_op | source)
XLA Modules:
  0.0 389.9 jit_solution(7729169001689056819)
XLA Ops:
  6.5 0.9 copy.81
  7.7 1.2 fusion.1
  9.0 0.6 reduce-window.6
  10.1 0.7 multiply_add_fusion
  10.8 0.8 convert_reduce_fusion.1
  11.7 1.4 convolution_convert_fusion.1
  13.1 1.5 reshape.57
  14.6 2.0 constant_dynamic-slice_fusion
  16.6 0.3 copy.85
  16.9 0.5 broadcast_in_dim.6
  17.4 0.3 broadcast_in_dim.14
  17.8 5.0 %all_to_all.20 = bf16[64,2,1,3,2048]{4,0,3,2,1:T(8,128)(2,1)S(1)} all-to-all(bf16[64,2,1,3,2048]{4,0,3,2,1:T(8,128)(2,1)S(1)} %broadcast_in_dim.15), channel_id=1, replica_groups=mesh['ep_0'=16,'ep_1'=4,'ep_2'=2,'tp'=4] {'ep_2'}, dimensions={1} | all-to-all | bytes 3145728 | tf_op jit(solution)/shard_map/all_to_all | solution.py:29
  22.8 1.6 copy.86
  24.5 96.4 %all_to_all.21 = bf16[64,2,1,3,2048]{4,1,3,2,0:T(2,128)(2,1)S(1)} all-to-all(bf16[64,2,1,3,2048]{4,1,3,2,0:T(2,128)(2,1)S(1)} %copy.86), channel_id=1, replica_groups=mesh['ep_0'=16,'ep_1'=4,'ep_2'=2,'tp'=4] {'ep_0','ep_1'}, dimensions={0} | all-to-all | bytes 3145728 | tf_op jit(solution)/shard_map/all_to_all | solution.py:29
  120.8 1.1 copy.87
  122.0 2.0 reshape_reshape.3
  124.0 0.2 all-gather.5.cloned.1.call-start
  124.3 65.0 %all-gather.3.cloned.1.call-done = bf16[128,12,2048]{2,0,1:T(8,128)(2,1)} async-done(((bf16[128,3,2048]{2,0,1:T(8,128)(2,1)}), bf16[128,12,2048]{2,0,1:T(8,128)(2,1)}) %all-gather.3.cloned.1.call-update) | async-done | bytes 6291472 | tf_op jit(solution)/shard_map/all_gather | solution.py:73
  189.3 9.7 %copy.88 = bf16[128,12,2048]{2,1,0:T(8,128)(2,1)} copy(bf16[128,12,2048]{2,0,1:T(8,128)(2,1)} %all-gather.3.cloned.1.call-done) | data formatting | bytes 12582912 | tf_op jit(solution)/shard_map/all_gather | solution.py:73
  198.9 10.8 %reshape.58 = bf16[1536,2048]{1,0:T(8,128)(2,1)} reshape(bf16[128,12,2048]{2,1,0:T(8,128)(2,1)} %copy.88) | data formatting | bytes 12582912 | tf_op jit(solution)/shard_map/reshape | solution.py:75
  209.7 4.8 %fusion.12 = f32[1536,256]{1,0:T(8,128)S(1)} fusion(bf16[1536,2048]{1,0:T(8,128)(2,1)} %reshape.58, bf16[2048,256]{1,0:T(8,128)(2,1)S(1)} %copy-done.3), kind=kOutput, calls=%fused_computation.30 | convolution fusion | flops 1610612736 | bytes 8912896 | tf_op jit(solution)/shard_map/dot_general | solution.py:76
  214.6 3.0 fusion
  217.6 51.2 %all-gather.5.cloned.1.call-done = bf16[1536,1024]{1,0:T(8,128)(2,1)} async-done(((bf16[1536,256]{1,0:T(8,128)(2,1)}), bf16[1536,1024]{1,0:T(8,128)(2,1)}) %all-gather.5.cloned.1.call-update) | async-done | bytes 3145744 | tf_op jit(solution)/shard_map/all_gather | solution.py:80
  268.8 4.8 %convolution_convert_fusion = bf16[1536,512]{1,0:T(8,128)(2,1)} fusion(bf16[1536,1024]{1,0:T(8,128)(2,1)} %all-gather.5.cloned.1.call-done, bf16[1024,512]{1,0:T(8,128)(2,1)S(1)} %copy-done), kind=kOutput, calls=%fused_computation.1 | convolution fusion | flops 1611399168 | bytes 5767168 | tf_op jit(solution)/shard_map/dot_general | solution.py:79
  273.6 2.4 reshape_reshape_reshape.2
  276.0 0.9 copy.89
  276.8 5.0 %all_to_all.22 = bf16[64,2,1,12,512]{4,0,3,2,1:T(8,128)(2,1)S(1)} all-to-all(bf16[64,2,1,12,512]{4,0,3,2,1:T(8,128)(2,1)S(1)} %copy.89), channel_id=1, replica_groups=mesh['ep_0'=16,'ep_1'=4,'ep_2'=2,'tp'=4] {'ep_2'}, dimensions={1} | all-to-all | bytes 3145728 | tf_op jit(solution)/shard_map/all_to_all | solution.py:29
  281.8 1.6 copy.90
  283.5 93.7 %all_to_all.23 = bf16[64,2,1,12,512]{4,1,3,2,0:T(2,128)(2,1)S(1)} all-to-all(bf16[64,2,1,12,512]{4,1,3,2,0:T(2,128)(2,1)S(1)} %copy.90), channel_id=1, replica_groups=mesh['ep_0'=16,'ep_1'=4,'ep_2'=2,'tp'=4] {'ep_0','ep_1'}, dimensions={0} | all-to-all | bytes 3145728 | tf_op jit(solution)/shard_map/all_to_all | solution.py:29
  377.1 4.2 %convert_reduce_fusion = f32[64,12,512]{2,1,0:T(8,128)S(1)} fusion(bf16[64,2,1,12,512]{4,1,3,2,0:T(2,128)(2,1)S(1)} %all_to_all.23), kind=kLoop, calls=%fused_computation | loop fusion | flops 1179648 | bytes 3145728 | tf_op jit(solution)/shard_map/reduce_sum | solution.py:86
  381.4 0.3 bitcast_reduce_fusion
  381.7 1.3 convolution_convert_fusion.2
  (25 shorter events, 1.2 us)
Async XLA Ops:
  6.5 262.3 %copy-start = (bf16[1024,512]{1,0:T(8,128)(2,1)S(1)}, bf16[1024,512]{1,0:T(8,128)(2,1)}, u32[]{:S(2)}) copy-start(bf16[1024,512]{1,0:T(8,128)(2,1)} %param.13) | copy-start | bytes 3145732
  6.5 5.1 %copy-start.2 = (bf16[128,2048]{1,0:T(8,128)(2,1)S(1)}, bf16[128,2048]{1,0:T(8,128)(2,1)}, u32[]{:S(2)}) copy-start(bf16[128,2048]{1,0:T(8,128)(2,1)} %param.7) | copy-start | bytes 1572868
  6.5 182.7 %all-gather.3.cloned.1.call-start = ((), (), s32[]{:S(2)}) async-start(), calls=%async_computation.4 | async-start | bytes 7864320 | tf_op jit(solution)/shard_map/all_gather | solution.py:73
  124.0 144.7 %all-gather.5.cloned.1.call-start = ((), (), s32[]{:S(2)}) async-start(), calls=%async_computation.5 | async-start | bytes 3932160 | tf_op jit(solution)/shard_map/all_gather | solution.py:80
  198.9 10.8 %copy-start.3 = (bf16[2048,256]{1,0:T(8,128)(2,1)S(1)}, bf16[2048,256]{1,0:T(8,128)(2,1)}, u32[]{:S(2)}) copy-start(bf16[2048,256]{1,0:T(8,128)(2,1)} %param.11) | copy-start | bytes 3145732
  209.7 4.8 %copy-start.1 = (bf16[1536,2048]{1,0:T(8,128)(2,1)S(1)}, bf16[1536,2048]{1,0:T(8,128)(2,1)}, u32[]{:S(2)}) copy-start(bf16[1536,2048]{1,0:T(8,128)(2,1)} %reshape.58) | copy-start | bytes 18874372
  209.7 4.9 %copy-start.4 = (bf16[2048,256]{1,0:T(8,128)(2,1)S(1)}, bf16[2048,256]{1,0:T(8,128)(2,1)}, u32[]{:S(2)}) copy-start(bf16[2048,256]{1,0:T(8,128)(2,1)} %param.12) | copy-start | bytes 3145732
Sparse Core Ops, SparseCore 0:
  124.2 65.0 all-gather.2
  217.7 51.0 all-gather.4
where the time goes:
time: 391 us; the launch traced here: 390 us
  blocking collectives  200 us (51%)
  waiting for transfers between devices  116 us (30%)
  local copies, waits for them, and re-layouts  36.5 us (9%)
  matrix products  15.2 us (4%)
  between operations  13.6 us (3%)
  other arithmetic  8.01 us (2%)
    all_to_all x4, blocking collectives, turned_blocks(): out = lax.all_to_all(out, axes[k], k, k, tiled=True)  200 us
    all_gather x1, waiting for transfers between devices, on_device(): received = lax.all_gather(arrived, 'tp', axis=1, tiled=True)  65 us
    all_gather x1, waiting for transfers between devices, on_device(): lax.all_gather(hidden, 'tp', axis=1, tiled=True)  51.2 us
    reshape x1, local copies, waits for them, and re-layouts, on_device(): flat_rows = received.reshape(sources * slot_count, model_width)  10.8 us
    all_gather x1, local copies, waits for them, and re-layouts, on_device(): received = lax.all_gather(arrived, 'tp', axis=1, tiled=True)  9.65 us
  transfers between devices with their start and end apart: 2, of which 2 were waited for; matrix products, arithmetic and copies ran while one was open for 0% of the time, Pallas kernels for 0%

commit v1 on v0

--- a/solution.py
+++ b/solution.py
@@ -8,6 +8,11 @@
 EP = ("ep_0", "ep_1", "ep_2")
 EP_TP = ("ep_0", "ep_1", "ep_2", "tp")
 EPS = 1e-06
+
+
+def gather_by_exchange(x, axis, dim):
+    copies = jnp.concatenate([x] * lax.axis_size(axis), axis=dim)
+    return lax.all_to_all(copies, axis, dim, dim, tiled=True)
 
 
 def split_up(array, dim, length):
@@ -70,7 +75,7 @@
     mine = lax.dynamic_slice_in_dim(buffers, lax.axis_index("tp") * quarter, quarter, 1)
     copies = jnp.repeat(mine, group_size, axis=0)
     arrived = exchange_by_chip(copies, (("ep_0", "ep_1"), "ep_2"), (1, 0), 0, 0)
-    received = lax.all_gather(arrived, "tp", axis=1, tiled=True)
+    received = gather_by_exchange(arrived, "tp", 1)
     sources, slot_count, model_width = received.shape
     flat_rows = received.reshape(sources * slot_count, model_width)
     gate_proj = jnp.dot(flat_rows, w_gate, preferred_element_type=jnp.float32)

time: 391 us -> 391 us (level)
  waiting for transfers between devices: 116 us -> 42.7 us
  blocking collectives: 200 us -> 273 us
  other arithmetic: 8.01 us -> 12.3 us
    all_to_all x0 -> x1, blocking collectives: none -> 72.9 us  [gather_by_exchange(): return lax.all_to_all(copies, axis, dim, dim, tiled=True)]
    all_gather x1 -> x0, waiting for transfers between devices: 65 us -> none  [on_device(): received = lax.all_gather(arrived, 'tp', axis=1, tiled=True)]
    all_gather x1 -> x0, local copies, waits for them, and re-layouts: 9.65 us -> none  [on_device(): received = lax.all_gather(arrived, 'tp', axis=1, tiled=True)]
    all_gather x1, waiting for transfers between devices: 51.2 us -> 42.6 us  [on_device(): lax.all_gather(hidden, 'tp', axis=1, tiled=True)]
    all_to_all x0 -> x1, local copies, waits for them, and re-layouts: none -> 6.85 us  [gather_by_exchange(): return lax.all_to_all(copies, axis, dim, dim, tiled=True)]
    concatenate x0 -> x1, other arithmetic: none -> 4.25 us  [gather_by_exchange(): copies = jnp.concatenate([x] * lax.axis_size(axis), axis=dim)]
  transfers between devices with their start and end apart: 2 -> 1, of which waited for: 2 -> 1; matrix products, arithmetic and copies ran while one was open for 0% -> 0% of each run, Pallas kernels for 0% -> 0%
where the time goes in v1:
time: 391 us
  blocking collectives  273 us (70%)
  waiting for transfers between devices  42.7 us (11%)
  local copies, waits for them, and re-layouts  33.7 us (9%)
  matrix products  15.6 us (4%)
  between operations  13.6 us (3%)
  other arithmetic  12.3 us (3%)
    all_to_all x4, blocking collectives, turned_blocks(): out = lax.all_to_all(out, axes[k], k, k, tiled=True)  200 us
    all_to_all x1, blocking collectives, gather_by_exchange(): return lax.all_to_all(copies, axis, dim, dim, tiled=True)  72.9 us
    all_gather x1, waiting for transfers between devices, on_device(): lax.all_gather(hidden, 'tp', axis=1, tiled=True)  42.6 us
    reshape x1, local copies, waits for them, and re-layouts, on_device(): flat_rows = received.reshape(sources * slot_count, model_width)  10.8 us
  transfers between devices with their start and end apart: 1, of which 1 were waited for; matrix products, arithmetic and copies ran while one was open for 0% of the time, Pallas kernels for 0%

profile of v1, /device:TPU:2, one launch (start us, length us, event | category | flops | bytes accessed | tf_op | source)
XLA Modules:
  0.0 390.6 jit_solution(8728948546626477701)
XLA Ops:
  6.5 0.9 copy.81
  7.7 1.2 fusion.1
  8.9 0.6 reduce-window.6
  10.1 0.7 multiply_add_fusion
  10.8 0.8 convert_reduce_fusion.1
  11.6 1.7 convolution_convert_fusion.1
  13.4 1.5 reshape.57
  14.9 2.0 constant_dynamic-slice_fusion
  16.9 0.3 copy.85
  17.2 0.5 broadcast_in_dim.6
  17.7 0.3 broadcast_in_dim.14
  18.1 5.0 %all_to_all.25 = bf16[64,2,1,3,2048]{4,0,3,2,1:T(8,128)(2,1)S(1)} all-to-all(bf16[64,2,1,3,2048]{4,0,3,2,1:T(8,128)(2,1)S(1)} %broadcast_in_dim.15), channel_id=1, replica_groups=mesh['ep_0'=16,'ep_1'=4,'ep_2'=2,'tp'=4] {'ep_2'}, dimensions={1} | all-to-all | bytes 3145728 | tf_op jit(solution)/shard_map/all_to_all | solution.py:34
  23.1 1.6 copy.86
  24.8 96.4 %all_to_all.26 = bf16[64,2,1,3,2048]{4,1,3,2,0:T(2,128)(2,1)S(1)} all-to-all(bf16[64,2,1,3,2048]{4,1,3,2,0:T(2,128)(2,1)S(1)} %copy.86), channel_id=1, replica_groups=mesh['ep_0'=16,'ep_1'=4,'ep_2'=2,'tp'=4] {'ep_0','ep_1'}, dimensions={0} | all-to-all | bytes 3145728 | tf_op jit(solution)/shard_map/all_to_all | solution.py:34
  121.2 1.1 copy.87
  122.3 2.0 reshape_reshape.3
  124.3 4.2 %pad_maximum_fusion = bf16[128,12,2048]{2,0,1:T(8,128)(2,1)S(1)} fusion(bf16[128,3,2048]{2,0,1:T(8,128)(2,1)} %reshape_reshape.3), kind=kLoop, calls=%fused_computation | loop fusion | flops 9437184 | bytes 7864320 | tf_op jit(solution)/shard_map/concatenate | solution.py:14
  128.6 72.9 %all_to_all.27 = bf16[128,12,2048]{2,0,1:T(8,128)(2,1)S(1)} all-to-all(bf16[128,12,2048]{2,0,1:T(8,128)(2,1)S(1)} %pad_maximum_fusion), channel_id=1, replica_groups=mesh['ep_0'=16,'ep_1'=4,'ep_2'=2,'tp'=4] {'tp'}, dimensions={1} | all-to-all | bytes 12582912 | tf_op jit(solution)/shard_map/all_to_all | solution.py:15
  201.4 6.9 %copy.88 = bf16[128,12,2048]{2,1,0:T(8,128)(2,1)} copy(bf16[128,12,2048]{2,0,1:T(8,128)(2,1)S(1)} %all_to_all.27) | data formatting | bytes 12582912 | tf_op jit(solution)/shard_map/all_to_all | solution.py:15
  208.3 10.8 %reshape.58 = bf16[1536,2048]{1,0:T(8,128)(2,1)} reshape(bf16[128,12,2048]{2,1,0:T(8,128)(2,1)} %copy.88) | data formatting | bytes 12582912 | tf_op jit(solution)/shard_map/reshape | solution.py:80
  219.1 4.8 %fusion.12 = f32[1536,256]{1,0:T(8,128)S(1)} fusion(bf16[1536,2048]{1,0:T(8,128)(2,1)} %reshape.58, bf16[2048,256]{1,0:T(8,128)(2,1)S(1)} %copy-done.2), kind=kOutput, calls=%fused_computation.31 | convolution fusion | flops 1610612736 | bytes 8912896 | tf_op jit(solution)/shard_map/dot_general | solution.py:81
  223.9 3.0 fusion
  226.9 42.6 %all-gather.2.cloned.1.call-done = bf16[1536,1024]{1,0:T(8,128)(2,1)} async-done(((bf16[1536,256]{1,0:T(8,128)(2,1)}), bf16[1536,1024]{1,0:T(8,128)(2,1)}) %all-gather.2.cloned.1.call-update) | async-done | bytes 3145744 | tf_op jit(solution)/shard_map/all_gather | solution.py:85
  269.5 4.8 %convolution_convert_fusion = bf16[1536,512]{1,0:T(8,128)(2,1)} fusion(bf16[1536,1024]{1,0:T(8,128)(2,1)} %all-gather.2.cloned.1.call-done, bf16[1024,512]{1,0:T(8,128)(2,1)S(1)} %copy-done), kind=kOutput, calls=%fused_computation.2 | convolution fusion | flops 1611399168 | bytes 5767168 | tf_op jit(solution)/shard_map/dot_general | solution.py:84
  274.4 2.4 reshape_reshape_reshape.2
  276.7 0.9 copy.89
  277.6 5.0 %all_to_all.28 = bf16[64,2,1,12,512]{4,0,3,2,1:T(8,128)(2,1)S(1)} all-to-all(bf16[64,2,1,12,512]{4,0,3,2,1:T(8,128)(2,1)S(1)} %copy.89), channel_id=1, replica_groups=mesh['ep_0'=16,'ep_1'=4,'ep_2'=2,'tp'=4] {'ep_2'}, dimensions={1} | all-to-all | bytes 3145728 | tf_op jit(solution)/shard_map/all_to_all | solution.py:34
  282.6 1.6 copy.90
  284.2 93.7 %all_to_all.29 = bf16[64,2,1,12,512]{4,1,3,2,0:T(2,128)(2,1)S(1)} all-to-all(bf16[64,2,1,12,512]{4,1,3,2,0:T(2,128)(2,1)S(1)} %copy.90), channel_id=1, replica_groups=mesh['ep_0'=16,'ep_1'=4,'ep_2'=2,'tp'=4] {'ep_0','ep_1'}, dimensions={0} | all-to-all | bytes 3145728 | tf_op jit(solution)/shard_map/all_to_all | solution.py:34
  377.9 4.2 %convert_reduce_fusion = f32[64,12,512]{2,1,0:T(8,128)S(1)} fusion(bf16[64,2,1,12,512]{4,1,3,2,0:T(2,128)(2,1)S(1)} %all_to_all.29), kind=kLoop, calls=%fused_computation.1 | loop fusion | flops 1179648 | bytes 3145728 | tf_op jit(solution)/shard_map/reduce_sum | solution.py:91
  382.1 0.3 bitcast_reduce_fusion
  382.5 1.3 convolution_convert_fusion.2
  (22 shorter events, 1.1 us)
Async XLA Ops:
  6.5 263.0 %copy-start = (bf16[1024,512]{1,0:T(8,128)(2,1)S(1)}, bf16[1024,512]{1,0:T(8,128)(2,1)}, u32[]{:S(2)}) copy-start(bf16[1024,512]{1,0:T(8,128)(2,1)} %param.13) | copy-start | bytes 3145732
  6.5 263.0 %all-gather.2.cloned.1.call-start = ((), (), s32[]{:S(2)}) async-start(), calls=%async_computation.5 | async-start | bytes 3932160 | tf_op jit(solution)/shard_map/all_gather | solution.py:85
  208.3 10.8 %copy-start.2 = (bf16[2048,256]{1,0:T(8,128)(2,1)S(1)}, bf16[2048,256]{1,0:T(8,128)(2,1)}, u32[]{:S(2)}) copy-start(bf16[2048,256]{1,0:T(8,128)(2,1)} %param.11) | copy-start | bytes 3145732
  219.1 4.8 %copy-start.1 = (bf16[1536,2048]{1,0:T(8,128)(2,1)S(1)}, bf16[1536,2048]{1,0:T(8,128)(2,1)}, u32[]{:S(2)}) copy-start(bf16[1536,2048]{1,0:T(8,128)(2,1)} %reshape.58) | copy-start | bytes 18874372
  219.1 4.9 %copy-start.3 = (bf16[2048,256]{1,0:T(8,128)(2,1)S(1)}, bf16[2048,256]{1,0:T(8,128)(2,1)}, u32[]{:S(2)}) copy-start(bf16[2048,256]{1,0:T(8,128)(2,1)} %param.12) | copy-start | bytes 3145732
Sparse Core Ops, SparseCore 0:
  227.0 42.4 all-gather.1
